TPU v7x, 32 devices: a whole 2x2x4 slice. The times are simulated.
32 devices in a mesh: fs: 4 (over y, x), tp: 8 (over z, core).
Axes of the slice: x: 2, y: 2, z: 4, core: 2. Of those that a mesh axis runs over, the one named last changes fastest.
Arguments:
- tokens: bfloat16 [2048, 2048], P('fs', 'tp'), may hold values from -6 to 6
- norm_gain: float32 [2048], P('fs'), may hold values from 0.1 to 1.9
- gate_train: float32 [2048, 8192], P('fs', 'tp'), may hold values from -0.125 to 0.125
- up_train: float32 [2048, 8192], P('fs', 'tp'), may hold values from -0.125 to 0.125
- down_train: float32 [8192, 2048], P('fs', 'tp'), may hold values from -0.0625 to 0.0625
Outputs:
- gate_serve: bfloat16 [2048, 8192], P(None, 'tp')
- up_serve: bfloat16 [2048, 8192], P(None, 'tp')
- down_serve: bfloat16 [8192, 2048], P('tp')
- layer_out: bfloat16 [2048, 2048], P(('fs', 'tp'))
All inputs are finite; a program needn't handle non-finite values.
Results may differ from a plain program's by a relative error of at most 0.024.
Values may be sent and summed in bfloat16 or wider, within the bound.
A program may use at most 64 MiB of HBM per device.

v0:
```python
import jax
import jax.numpy as jnp
from jax import lax
from jax.sharding import PartitionSpec as P

D = 2048
epsilon = 1e-06


def body(tokens, norm_gain, gate_train, up_train, down_train):
    gate_local = (norm_gain[:, None] * gate_train).astype(jnp.bfloat16)
    up_local = (norm_gain[:, None] * up_train).astype(jnp.bfloat16)
    down_local = down_train.astype(jnp.bfloat16)
    features = lax.all_gather(tokens, "tp", axis=1, tiled=True)
    wide = features.astype(jnp.float32)
    squares = jnp.sum(wide * wide, axis=1)
    gate_whole, up_whole = (
        lax.all_gather(gate_local, "fs", axis=0, tiled=True),
        lax.all_gather(up_local, "fs", axis=0, tiled=True),
    )
    gate_sum = jnp.dot(features, gate_whole, preferred_element_type=jnp.float32)
    up_sum = jnp.dot(features, up_whole, preferred_element_type=jnp.float32)
    down_rows = lax.all_gather(down_local, "fs", axis=0, tiled=True)
    down_whole = lax.all_to_all(down_rows, "tp", split_axis=0, concat_axis=1, tiled=True)
    scale = lax.rsqrt(squares / D + epsilon)[:, None]
    hidden = (jax.nn.silu(gate_sum * scale) * (up_sum * scale)).astype(jnp.bfloat16)
    mixed = lax.psum_scatter(
        jnp.dot(hidden, down_whole, preferred_element_type=jnp.float32).astype(jnp.bfloat16),
        "tp",
        scatter_dimension=0,
        tiled=True,
    )
    return (gate_whole, up_whole, down_whole, mixed)


def solution(mesh):
    return jax.shard_map(
        body,
        mesh=mesh,
        in_specs=(P("fs", "tp"), P("fs"), P("fs", "tp"), P("fs", "tp"), P("fs", "tp")),
        out_specs=(P(None, "tp"), P(None, "tp"), P("tp", None), P(("fs", "tp"), None)),
        check_vma=False,
    )
```

profile of v0, /device:TPU:0, one launch (start us, length us, event | category | flops | bytes accessed | tf_op | source)
XLA Modules:
  0.0 293.7 jit_solution(2137613969868247611)
XLA Ops:
  7.2 0.0 all-gather.9.cloned.1.call-start
  7.2 2.8 convert_element_type.20
  10.0 0.0 all-gather.9.cloned.1.call-update
  10.1 0.0 all-gather.11.cloned.1.call-start
  10.1 0.7 all-gather.11.cloned.1.call-update
  10.8 0.0 all-gather.5.cloned.1.call-start
  10.9 3.2 %multiply_convert_fusion = (bf16[512,1024]{1,0:T(8,128)(2,1)}, bf16[512,1024]{1,0:T(8,128)(2,1)}) fusion(f32[512,1024]{1,0:T(8,128)S(1)} %copy-done.2, f32[512]{0:T(512)S(1)} %copy-done.3, f32[512,1024]{1,0:T(8,128)} %param.7), kind=kLoop, calls=%fused_computation.9 | loop fusion | flops 2097152 | bytes 6293504 | tf_op jit(solution)/shard_map/convert_element_type | solution.py:12
  14.1 0.0 all-gather.5.cloned.1.call-update
  14.1 51.6 %all-gather.9.cloned.1.call-done = bf16[8192,256]{1,0:T(8,128)(2,1)} async-done(((bf16[2048,256]{1,0:T(8,128)(2,1)}), bf16[8192,256]{1,0:T(8,128)(2,1)}) %all-gather.9.cloned.1.call-update) | async-done | bytes 4194320 | tf_op jit(solution)/shard_map/all_gather | solution.py:23
  65.7 4.6 %all-to-all-start = ((bf16[8,1024,256]{2,1,0:T(8,128)(2,1)}), bf16[8,1024,256]{2,1,0:T(8,128)(2,1)}, u32[]{:S(2)}, u32[]{:S(2)}) async-start(bf16[8,1024,256]{2,1,0:T(8,128)(2,1)} %bitcast.32), calls=%async_computation | async-start | bytes 8388608 | tf_op jit(solution)/shard_map/all_to_all | solution.py:24
  70.3 0.0 all-gather.7.cloned.1.call-start
  70.4 0.5 all-gather.7.cloned.1.call-update
  70.9 0.0 reduce-scatter.2.cloned.1.call-start
  71.0 50.9 %all-gather.11.cloned.1.call-done = bf16[512,2048]{1,0:T(8,128)(2,1)} async-done(((bf16[512,256]{1,0:T(8,128)(2,1)}), bf16[512,2048]{1,0:T(8,128)(2,1)}) %all-gather.11.cloned.1.call-update) | async-done | bytes 2097168 | tf_op jit(solution)/shard_map/all_gather | solution.py:14
  121.8 2.2 multiply_reduce_fusion
  124.1 54.8 %all-gather.5.cloned.1.call-done = bf16[2048,1024]{1,0:T(8,128)(2,1)} async-done(((bf16[512,1024]{1,0:T(8,128)(2,1)}), bf16[2048,1024]{1,0:T(8,128)(2,1)}) %all-gather.5.cloned.1.call-update) | async-done | bytes 4194320 | tf_op jit(solution)/shard_map/all_gather | solution.py:18
  178.9 5.9 %fusion.5 = f32[1024,512]{1,0:T(8,128)} fusion(bf16[2048,1024]{1,0:T(8,128)(2,1)} %all-gather.5.cloned.1.call-done, bf16[512,2048]{1,0:T(8,128)(2,1)S(1)} %copy-done.1), kind=kOutput, calls=%fused_computation.13 | convolution fusion | flops 2147483648 | bytes 8388608 | tf_op jit(solution)/shard_map/dot_general | solution.py:21
  184.8 6.5 %copy.10 = bf16[8,1024,256]{1,2,0:T(8,128)(2,1)} copy(bf16[8,1024,256]{2,1,0:T(8,128)(2,1)} %all-to-all-done) | data formatting | bytes 8388608 | tf_op jit(solution)/shard_map/all_to_all | solution.py:24
  191.2 42.5 %all-gather.7.cloned.1.call-done = bf16[2048,1024]{1,0:T(8,128)(2,1)} async-done(((bf16[512,1024]{1,0:T(8,128)(2,1)}), bf16[2048,1024]{1,0:T(8,128)(2,1)}) %all-gather.7.cloned.1.call-update) | async-done | bytes 4194320 | tf_op jit(solution)/shard_map/all_gather | solution.py:19
  233.7 10.3 %convolution_convert_fusion = bf16[512,2048]{1,0:T(8,128)(2,1)} fusion(bf16[1024,2048]{0,1:T(8,128)(2,1)} %bitcast.30, f32[1024,512]{1,0:T(8,128)} %fusion.5, bf16[2048,1024]{1,0:T(8,128)(2,1)} %all-gather.7.cloned.1.call-done, bf16[512,2048]{1,0:T(8,128)(2,1)S(1)} %copy-done.1, f32[512]{0:T(512)S(1)} %add_rsqrt_fusion), kind=kOutput, calls=%fused_computation.1 | convolution fusion | flops 4300210176 | bytes 14682112 | tf_op jit(solution)/shard_map/dot_general | solution.py:28
  244.0 6.4 %copy.11 = bf16[1024,2048]{1,0:T(8,128)(2,1)} copy(bf16[1024,2048]{0,1:T(8,128)(2,1)} %bitcast.31) | data formatting | bytes 8388608
  250.5 29.8 %reduce-scatter.2.cloned.1.call-done = bf16[64,2048]{1,0:T(8,128)(2,1)} async-done(((bf16[512,2048]{1,0:T(8,128)(2,1)}), bf16[64,2048]{1,0:T(8,128)(2,1)}) %reduce-scatter.2.cloned.1.call-update) | async-done | bytes 262160 | tf_op jit(solution)/shard_map/reduce_scatter | solution.py:27
  280.3 4.8 %copy.14 = bf16[2048,1024]{1,0:T(8,128)(2,1)} copy(bf16[2048,1024]{1,0:T(8,128)(2,1)} %all-gather.5.cloned.1.call-done) | data formatting | bytes 8388608
  285.1 2.0 copy.15
  (11 shorter events, 0.0 us)
Async XLA Ops:
  7.2 3.7 %copy-start.2 = (f32[512,1024]{1,0:T(8,128)S(1)}, f32[512,1024]{1,0:T(8,128)}, u32[]{:S(2)}) copy-start(f32[512,1024]{1,0:T(8,128)} %param.8) | copy-start | bytes 6291460
  7.2 3.7 %copy-start.3 = (f32[512]{0:T(512)S(1)}, f32[512]{0:T(512)}, u32[]{:S(2)}) copy-start(f32[512]{0:T(512)} %param.6) | copy-start | bytes 6148
  7.2 58.6 %all-gather.9.cloned.1.call-start = ((), (), s32[]{:S(2)}) async-start(), calls=%async_computation.4 | async-start | bytes 5242880 | tf_op jit(solution)/shard_map/all_gather | solution.py:23
  10.1 111.8 %all-gather.11.cloned.1.call-start = ((), (), s32[]{:S(2)}) async-start(), calls=%async_computation.5 | async-start | bytes 2359296 | tf_op jit(solution)/shard_map/all_gather | solution.py:14
  10.8 168.1 %all-gather.5.cloned.1.call-start = ((), (), s32[]{:S(2)}) async-start(), calls=%async_computation.2 | async-start | bytes 5242880 | tf_op jit(solution)/shard_map/all_gather | solution.py:18
  65.7 119.0 %all-to-all-start = ((bf16[8,1024,256]{2,1,0:T(8,128)(2,1)}), bf16[8,1024,256]{2,1,0:T(8,128)(2,1)}, u32[]{:S(2)}, u32[]{:S(2)}) async-start(bf16[8,1024,256]{2,1,0:T(8,128)(2,1)} %bitcast.32), calls=%async_computation | async-start | bytes 8388608 | tf_op jit(solution)/shard_map/all_to_all | solution.py:24
  70.3 163.4 %all-gather.7.cloned.1.call-start = ((), (), s32[]{:S(2)}) async-start(), calls=%async_computation.3 | async-start | bytes 5242880 | tf_op jit(solution)/shard_map/all_gather | solution.py:19
  70.9 209.4 %reduce-scatter.2.cloned.1.call-start = ((), (), s32[]{:S(2)}) async-start(), calls=%async_computation.6 | async-start | bytes 2359296 | tf_op jit(solution)/shard_map/reduce_scatter | solution.py:27
  121.8 57.0 %copy-start.1 = (bf16[512,2048]{1,0:T(8,128)(2,1)S(1)}, bf16[512,2048]{1,0:T(8,128)(2,1)}, u32[]{:S(2)}) copy-start(bf16[512,2048]{1,0:T(8,128)(2,1)} %all-gather.11.cloned.1.call-done) | copy-start | bytes 6291460
  280.3 4.8 %copy-start = (bf16[2048,1024]{1,0:T(8,128)(2,1)S(1)}, bf16[2048,1024]{1,0:T(8,128)(2,1)}, u32[]{:S(2)}) copy-start(bf16[2048,1024]{1,0:T(8,128)(2,1)} %all-gather.7.cloned.1.call-done) | copy-start | bytes 12582916
Sparse Core Ops, SparseCore 0:
  10.4 55.2 all-gather.8
  67.3 54.4 all-gather.10
  124.3 54.5 all-gather.4
  181.1 52.5 all-gather.6
  244.2 36.0 reduce-scatter.1
where the time goes:
time: 294 us
  waiting for transfers between devices  231 us (79%)
  local copies, waits for them, and re-layouts  19.8 us (7%)
  matrix products  16.2 us (6%)
  between operations  13.8 us (5%)
  other arithmetic  8.23 us (3%)
  starting transfers between devices  4.8 us (2%)
    all_gather x1, waiting for transfers between devices, body(): lax.all_gather(gate_local, 'fs', axis=0, tiled=True)  54.8 us
    all_gather x1, waiting for transfers between devices, body(): down_rows = lax.all_gather(down_local, 'fs', axis=0, tiled=True)  51.6 us
    all_gather x1, waiting for transfers between devices, body(): features = lax.all_gather(tokens, 'tp', axis=1, tiled=True)  50.9 us
    all_gather x1, waiting for transfers between devices, body(): lax.all_gather(up_local, 'fs', axis=0, tiled=True)  42.5 us
    reduce_scatter x1, waiting for transfers between devices, body(): lax.psum_scatter(jnp.dot(hidden, down_whole, preferred_element_type=jnp.f...  29.8 us
    unnamed x11, local copies, waits for them, and re-layouts  13.3 us
    dot_general x1, matrix products, body(): jnp.dot(hidden, down_whole, preferred_element_type=jnp.float32)  10.3 us
    all_to_all x1, local copies, waits for them, and re-layouts, body(): lax.all_to_all(down_rows, 'tp', split_axis=0, concat_axis=1, tiled=True)  6.48 us
  transfers between devices with their start and end apart: 6, of which 5 were waited for; matrix products, arithmetic and copies ran while one was open for 8% of the time, Pallas kernels for 0%

commit v1 on v0

--- a/solution.py
+++ b/solution.py
@@ -5,6 +5,24 @@
 
 D = 2048
 epsilon = 1e-06
+
+
+def replace_heads(dev_axis, row_data):
+    num = lax.axis_size(dev_axis)
+    tmp = map(lambda j: (j, (j + 1) % num), range(num))
+    log = list(tmp)
+    val2 = map(lambda j: (j, (j - 1) % num), range(num))
+    pool = list(val2)
+    front, after = ([row_data], [row_data])
+    for _ in range(num // 2):
+        front.append(lax.ppermute(front[-1], dev_axis, log))
+    w = 0
+    while w < (num - 1) // 2:
+        after.append(lax.ppermute(after[-1], dev_axis, pool))
+        w = w + 1
+    a_next = jnp.concatenate([*front[::-1], *after[1:]], axis=0)
+    high = jnp.roll(a_next, (lax.axis_index(dev_axis) - num // 2) * row_data.shape[0], axis=0)
+    return high
 
 
 def body(tokens, norm_gain, gate_train, up_train, down_train):
@@ -16,7 +34,7 @@
     squares = jnp.sum(wide * wide, axis=1)
     gate_whole, up_whole = (
         lax.all_gather(gate_local, "fs", axis=0, tiled=True),
-        lax.all_gather(up_local, "fs", axis=0, tiled=True),
+        replace_heads("fs", row_data=up_local),
     )
     gate_sum = jnp.dot(features, gate_whole, preferred_element_type=jnp.float32)
     up_sum = jnp.dot(features, up_whole, preferred_element_type=jnp.float32)

time: 294 us -> 260 us (0.88)
  waiting for transfers between devices: 231 us -> 188 us
  starting transfers between devices: 4.8 us -> 9.34 us
  local copies, waits for them, and re-layouts: 19.8 us -> 23.1 us
    ppermute x0 -> x3, waiting for transfers between devices: none -> 79.9 us  [the longest x2 49.1 us: replace_heads(): front.append(lax.ppermute(front[-1], dev_axis, log))]
    all_gather x1, waiting for transfers between devices: 50.9 us -> 0.01 us  [body(): features = lax.all_gather(tokens, 'tp', axis=1, tiled=True)]
    all_gather x1 -> x0, waiting for transfers between devices: 42.5 us -> none  [body(): lax.all_gather(up_local, 'fs', axis=0, tiled=True)]
    all_gather x1, waiting for transfers between devices: 54.8 us -> 22.7 us  [body(): lax.all_gather(gate_local, 'fs', axis=0, tiled=True)]
    ppermute x0 -> x3, starting transfers between devices: none -> 4.45 us  [the longest x1 2.36 us: replace_heads(): after.append(lax.ppermute(after[-1], dev_axis, pool))]
    all_gather x1, waiting for transfers between devices: 51.6 us -> 55.1 us  [body(): down_rows = lax.all_gather(down_local, 'fs', axis=0, tiled=True)]
    unnamed x11 -> x15, local copies, waits for them, and re-layouts: 13.3 us -> 14 us
  transfers between devices with their start and end apart: 6 -> 8, of which waited for: 5 -> 6; matrix products, arithmetic and copies ran while one was open for 8% -> 9% of each run, Pallas kernels for 0% -> 0%
where the time goes in v1:
time: 260 us
  waiting for transfers between devices  188 us (72%)
  local copies, waits for them, and re-layouts  23.1 us (9%)
  matrix products  16.9 us (6%)
  between operations  13.8 us (5%)
  starting transfers between devices  9.34 us (4%)
  other arithmetic  8.21 us (3%)
    all_gather x1, waiting for transfers between devices, body(): down_rows = lax.all_gather(down_local, 'fs', axis=0, tiled=True)  55.1 us
    ppermute x2, waiting for transfers between devices, replace_heads(): front.append(lax.ppermute(front[-1], dev_axis, log))  49.1 us
    ppermute x1, waiting for transfers between devices, replace_heads(): after.append(lax.ppermute(after[-1], dev_axis, pool))  30.9 us
    reduce_scatter x1, waiting for transfers between devices, body(): lax.psum_scatter(jnp.dot(hidden, down_whole, preferred_element_type=jnp.f...  29.7 us
    all_gather x1, waiting for transfers between devices, body(): lax.all_gather(gate_local, 'fs', axis=0, tiled=True)  22.7 us
    unnamed x15, local copies, waits for them, and re-layouts  14 us
    dot_general x1, matrix products, body(): jnp.dot(hidden, down_whole, preferred_element_type=jnp.float32)  10.3 us
    all_to_all x1, local copies, waits for them, and re-layouts, body(): lax.all_to_all(down_rows, 'tp', split_axis=0, concat_axis=1, tiled=True)  6.58 us
  transfers between devices with their start and end apart: 8, of which 6 were waited for; matrix products, arithmetic and copies ran while one was open for 9% of the time, Pallas kernels for 0%

profile of v1, /device:TPU:0, one launch (start us, length us, event | category | flops | bytes accessed | tf_op | source)
XLA Modules:
  0.0 259.5 jit_solution(3246727897130950576)
XLA Ops:
  7.2 2.7 %convert_element_type.20 = bf16[2048,256]{1,0:T(8,128)(2,1)} convert(f32[2048,256]{1,0:T(8,128)} %param.9) | non-fusion elementwise | flops 524288 | bytes 3145728 | tf_op jit(solution)/shard_map/convert_element_type | solution.py:31
  9.9 0.7 all-gather.8.cloned.1.call-update
  10.7 55.1 %all-gather.6.cloned.1.call-done = bf16[8192,256]{1,0:T(8,128)(2,1)} async-done(((bf16[2048,256]{1,0:T(8,128)(2,1)}), bf16[8192,256]{1,0:T(8,128)(2,1)}) %all-gather.6.cloned.1.call-update) | async-done | bytes 4194320 | tf_op jit(solution)/shard_map/all_gather | solution.py:41
  65.7 4.7 %all-to-all-start = ((bf16[8,1024,256]{2,1,0:T(8,128)(2,1)}), bf16[8,1024,256]{2,1,0:T(8,128)(2,1)}, u32[]{:S(2)}, u32[]{:S(2)}) async-start(bf16[8,1024,256]{2,1,0:T(8,128)(2,1)} %bitcast.32), calls=%async_computation | async-start | bytes 8388608 | tf_op jit(solution)/shard_map/all_to_all | solution.py:42
  70.5 2.9 %multiply_convert_fusion = (bf16[512,1024]{1,0:T(8,128)(2,1)S(1)}, bf16[512,1024]{1,0:T(8,128)(2,1)}) fusion(f32[512,1024]{1,0:T(8,128)S(1)} %copy-done.1, f32[512]{0:T(512)S(1)} %copy-done.2, f32[512,1024]{1,0:T(8,128)} %param.7), kind=kLoop, calls=%fused_computation.9 | loop fusion | flops 2097152 | bytes 6293504 | tf_op jit(solution)/shard_map/convert_element_type | solution.py:30
  73.5 1.5 collective-permute-start
  75.0 25.0 %collective-permute-done = bf16[512,1024]{1,0:T(8,128)(2,1)S(1)} collective-permute-done((bf16[512,1024]{1,0:T(8,128)(2,1)S(1)}, bf16[512,1024]{1,0:T(8,128)(2,1)S(1)}, u32[]{:S(2)}, u32[]{:S(2)}) %collective-permute-start) | collective-permute-done | bytes 1048608 | tf_op jit(solution)/shard_map/ppermute | solution.py:18
  99.9 0.6 collective-permute-start.1
  100.5 2.4 collective-permute-start.2
  102.9 24.1 %collective-permute-done.1 = bf16[512,1024]{1,0:T(8,128)(2,1)} collective-permute-done((bf16[512,1024]{1,0:T(8,128)(2,1)S(1)}, bf16[512,1024]{1,0:T(8,128)(2,1)}, u32[]{:S(2)}, u32[]{:S(2)}) %collective-permute-start.1) | collective-permute-done | bytes 1048608 | tf_op jit(solution)/shard_map/ppermute | solution.py:18
  127.0 1.3 constant_dynamic-update-slice_fusion.7
  128.3 0.1 constant_dynamic-update-slice_fusion.6
  128.3 0.1 constant_dynamic-update-slice_fusion.5
  128.4 30.9 %collective-permute-done.2 = bf16[512,1024]{1,0:T(8,128)(2,1)S(1)} collective-permute-done((bf16[512,1024]{1,0:T(8,128)(2,1)S(1)}, bf16[512,1024]{1,0:T(8,128)(2,1)S(1)}, u32[]{:S(2)}, u32[]{:S(2)}) %collective-permute-start.2) | collective-permute-done | bytes 1048608 | tf_op jit(solution)/shard_map/ppermute | solution.py:21
  159.4 1.3 constant_dynamic-update-slice_fusion.3
  160.9 2.5 constant_dynamic-slice_fusion
  163.4 2.7 %multiply_reduce_fusion = f32[512]{0:T(512)S(1)} fusion(bf16[512,2048]{1,0:T(8,128)(2,1)} %all-gather.8.cloned.1.call-done), kind=kLoop, calls=%fused_computation | loop fusion | flops 3145216 | bytes 2099200 | tf_op jit(solution)/shard_map/reduce_sum | solution.py:34
  166.1 22.7 %all-gather.4.cloned.1.call-done = bf16[2048,1024]{1,0:T(8,128)(2,1)} async-done(((bf16[512,1024]{1,0:T(8,128)(2,1)}), bf16[2048,1024]{1,0:T(8,128)(2,1)}) %all-gather.4.cloned.1.call-update) | async-done | bytes 4194320 | tf_op jit(solution)/shard_map/all_gather | solution.py:36
  188.8 6.6 %fusion.5 = f32[1024,512]{1,0:T(8,128)} fusion(bf16[2048,1024]{1,0:T(8,128)(2,1)} %all-gather.4.cloned.1.call-done, bf16[512,2048]{1,0:T(8,128)(2,1)} %all-gather.8.cloned.1.call-done), kind=kOutput, calls=%fused_computation.22 | convolution fusion | flops 2147483648 | bytes 8388608 | tf_op jit(solution)/shard_map/dot_general | solution.py:39
  195.3 6.6 %copy.10 = bf16[8,1024,256]{1,2,0:T(8,128)(2,1)} copy(bf16[8,1024,256]{2,1,0:T(8,128)(2,1)} %all-to-all-done) | data formatting | bytes 8388608 | tf_op jit(solution)/shard_map/all_to_all | solution.py:42
  201.9 10.3 %convolution_convert_fusion = bf16[512,2048]{1,0:T(8,128)(2,1)} fusion(bf16[1024,2048]{0,1:T(8,128)(2,1)} %bitcast.30, f32[1024,512]{1,0:T(8,128)} %fusion.5, bf16[2048,1024]{1,0:T(8,128)(2,1)} %constant_dynamic-slice_fusion, bf16[512,2048]{1,0:T(8,128)(2,1)S(1)} %copy-done, f32[512]{0:T(512)S(1)} %add_rsqrt_fusion), kind=kOutput, calls=%fused_computation.1 | convolution fusion | flops 4300210176 | bytes 14682112 | tf_op jit(solution)/shard_map/dot_general | solution.py:46
  212.2 6.4 %copy.11 = bf16[1024,2048]{1,0:T(8,128)(2,1)} copy(bf16[1024,2048]{0,1:T(8,128)(2,1)} %bitcast.31) | data formatting | bytes 8388608
  218.7 29.7 %reduce-scatter.2.cloned.1.call-done = bf16[64,2048]{1,0:T(8,128)(2,1)} async-done(((bf16[512,2048]{1,0:T(8,128)(2,1)}), bf16[64,2048]{1,0:T(8,128)(2,1)}) %reduce-scatter.2.cloned.1.call-update) | async-done | bytes 262160 | tf_op jit(solution)/shard_map/reduce_scatter | solution.py:45
  248.3 4.6 %copy.20 = bf16[2048,1024]{1,0:T(8,128)(2,1)} copy(bf16[2048,1024]{1,0:T(8,128)(2,1)} %all-gather.4.cloned.1.call-done) | data formatting | bytes 8388608
  (20 shorter events, 0.5 us)
Async XLA Ops:
  7.2 58.6 %all-gather.6.cloned.1.call-start = ((), (), s32[]{:S(2)}) async-start(), calls=%async_computation.3 | async-start | bytes 5242880 | tf_op jit(solution)/shard_map/all_gather | solution.py:41
  9.9 153.5 %all-gather.8.cloned.1.call-start = ((), (), s32[]{:S(2)}) async-start(), calls=%async_computation.4 | async-start | bytes 2359296 | tf_op jit(solution)/shard_map/all_gather | solution.py:32
  65.7 4.8 %copy-start.1 = (f32[512,1024]{1,0:T(8,128)S(1)}, f32[512,1024]{1,0:T(8,128)}, u32[]{:S(2)}) copy-start(f32[512,1024]{1,0:T(8,128)} %param.8) | copy-start | bytes 6291460
  65.7 4.8 %copy-start.2 = (f32[512]{0:T(512)S(1)}, f32[512]{0:T(512)}, u32[]{:S(2)}) copy-start(f32[512]{0:T(512)} %param.6) | copy-start | bytes 6148
  65.7 129.6 %all-to-all-start = ((bf16[8,1024,256]{2,1,0:T(8,128)(2,1)}), bf16[8,1024,256]{2,1,0:T(8,128)(2,1)}, u32[]{:S(2)}, u32[]{:S(2)}) async-start(bf16[8,1024,256]{2,1,0:T(8,128)(2,1)} %bitcast.32), calls=%async_computation | async-start | bytes 8388608 | tf_op jit(solution)/shard_map/all_to_all | solution.py:42
  70.5 118.3 %all-gather.4.cloned.1.call-start = ((), (), s32[]{:S(2)}) async-start(), calls=%async_computation.2 | async-start | bytes 5242880 | tf_op jit(solution)/shard_map/all_gather | solution.py:36
  73.4 174.9 %reduce-scatter.2.cloned.1.call-start = ((), (), s32[]{:S(2)}) async-start(), calls=%async_computation.5 | async-start | bytes 2359296 | tf_op jit(solution)/shard_map/reduce_scatter | solution.py:45
  73.5 26.5 %collective-permute-start = (bf16[512,1024]{1,0:T(8,128)(2,1)S(1)}, bf16[512,1024]{1,0:T(8,128)(2,1)S(1)}, u32[]{:S(2)}, u32[]{:S(2)}) collective-permute-start(bf16[512,1024]{1,0:T(8,128)(2,1)S(1)} %get-tuple-element.8), channel_id=1, source_target_pairs={{0,8},{8,16},{16,24},{24,0},{1,9},{9,17},{17,25},{25,1},{2,10},{10... | collective-permute-start | bytes 3145736 | tf_op jit(solution)/shard_map/ppermute | solution.py:18
  99.9 27.0 %collective-permute-start.1 = (bf16[512,1024]{1,0:T(8,128)(2,1)S(1)}, bf16[512,1024]{1,0:T(8,128)(2,1)}, u32[]{:S(2)}, u32[]{:S(2)}) collective-permute-start(bf16[512,1024]{1,0:T(8,128)(2,1)S(1)} %collective-permute-done), channel_id=1, source_target_pairs={{0,8},{8,16},{16,24},{24,0},{1,9},{9,17},{17,25},{25,1},{2,10},{10... | collective-permute-start | bytes 3145736 | tf_op jit(solution)/shard_map/ppermute | solution.py:18
  100.5 58.8 %collective-permute-start.2 = (bf16[512,1024]{1,0:T(8,128)(2,1)S(1)}, bf16[512,1024]{1,0:T(8,128)(2,1)S(1)}, u32[]{:S(2)}, u32[]{:S(2)}) collective-permute-start(bf16[512,1024]{1,0:T(8,128)(2,1)S(1)} %get-tuple-element.8), channel_id=1, source_target_pairs={{0,24},{8,0},{16,8},{24,16},{1,25},{9,1},{17,9},{25,17},{2,26},{10... | collective-permute-start | bytes 3145736 | tf_op jit(solution)/shard_map/ppermute | solution.py:21
  195.3 6.6 %copy-start = (bf16[512,2048]{1,0:T(8,128)(2,1)S(1)}, bf16[512,2048]{1,0:T(8,128)(2,1)}, u32[]{:S(2)}) copy-start(bf16[512,2048]{1,0:T(8,128)(2,1)} %all-gather.8.cloned.1.call-done) | copy-start | bytes 6291460
Sparse Core Ops, SparseCore 0:
  10.4 55.2 all-gather.5
  67.3 54.5 all-gather.7
  124.3 64.3 all-gather.3
  212.4 35.9 reduce-scatter.1
